TPU v7x, 32 devices: a whole 2x2x4 slice. The times are simulated.
32 devices in a mesh: fs: 4 (over y, x), tp: 8 (over z, core).
Axes of the slice: x: 2, y: 2, z: 4, core: 2. Of those that a mesh axis runs over, the one named last changes fastest.
Arguments:
- tokens: bfloat16 [4096, 2048], P(('fs', 'tp')), may hold values from -6 to 6
- norm_gain: float32 [2048], replicated, may hold values from 0.1 to 1.9
- gate_weight: bfloat16 [2048, 5632], P('fs', 'tp'), may hold values from -0.125 to 0.125
- up_weight: bfloat16 [2048, 5632], P('fs', 'tp'), may hold values from -0.125 to 0.125
- down_weight: bfloat16 [5632, 2048], P('tp', 'fs'), may hold values from -0.078125 to 0.078125
Outputs:
- mixed: bfloat16 [4096, 2048], P(('fs', 'tp'))
All inputs are finite; a program needn't handle non-finite values.
Results may differ from a plain program's by a relative error of at most 0.0065.
Values may be sent and summed in bfloat16 or wider, within the bound.
A program may use at most 128 MiB of HBM per device.

v0:
```python
import jax
import jax.numpy as jnp
from jax import lax
from jax.sharding import PartitionSpec as P

eps_floor = 0.05


def local(tokens, norm_gain, gate_weight, up_weight, down_weight):
    values = tokens.astype(jnp.float32)
    factor = lax.rsqrt(jnp.mean(values * values, axis=-1, keepdims=True) + eps_floor)
    normed = (values * factor * norm_gain).astype(jnp.bfloat16)
    local_ff = gate_weight.shape[1]
    group = lax.all_gather(normed, "tp", axis=0, tiled=True)
    joined = jnp.concatenate(
        (
            lax.all_gather(gate_weight, "fs", axis=0, tiled=True),
            lax.all_gather(up_weight, "fs", axis=0, tiled=True),
        ),
        axis=1,
    )
    product = jnp.dot(group, joined, preferred_element_type=jnp.float32)
    hidden = (jax.nn.silu(product[:, :local_ff]) * product[:, local_ff:]).astype(jnp.bfloat16)
    down_local = lax.all_gather(down_weight, "fs", axis=1, tiled=True)
    mixed = lax.psum_scatter(
        jnp.dot(hidden, down_local, preferred_element_type=jnp.float32),
        "tp",
        scatter_dimension=0,
        tiled=True,
    )
    return mixed.astype(jnp.bfloat16)


def solution(mesh):
    return jax.shard_map(
        local,
        mesh=mesh,
        in_specs=(P(("fs", "tp"), None), P(), P("fs", "tp"), P("fs", "tp"), P("tp", "fs")),
        out_specs=P(("fs", "tp"), None),
        check_vma=False,
    )
```

profile of v0, /device:TPU:0, one launch (start us, length us, event | category | flops | bytes accessed | tf_op | source)
XLA Modules:
  0.0 296.1 jit_solution(4076748041551358290)
XLA Ops:
  6.5 0.0 all-gather.7.cloned.1.call-start
  6.5 0.7 all-gather.7.cloned.1.call-update
  7.3 0.0 all-gather.9.cloned.1.call-start
  7.3 0.7 all-gather.9.cloned.1.call-update
  8.0 0.0 all-gather.5.cloned.1.call-start
  8.1 1.2 fusion.8
  9.3 2.0 fusion.10
  11.3 0.0 all-gather.5.cloned.1.call-update
  11.3 0.0 all-gather.11.cloned.1.call-start
  11.4 0.5 all-gather.11.cloned.1.call-update
  11.9 0.0 reduce-scatter.2.cloned.1.call-start
  12.0 41.5 %all-gather.7.cloned.1.call-done = bf16[2048,704]{0,1:T(8,128)(2,1)} async-done(((bf16[512,704]{0,1:T(8,128)(2,1)}), bf16[2048,704]{0,1:T(8,128)(2,1)}) %all-gather.7.cloned.1.call-update) | async-done | bytes 2883600 | tf_op jit(solution)/shard_map/all_gather | solution.py:17
  53.5 43.4 %all-gather.9.cloned.1.call-done = bf16[2048,704]{0,1:T(8,128)(2,1)} async-done(((bf16[512,704]{0,1:T(8,128)(2,1)}), bf16[2048,704]{0,1:T(8,128)(2,1)}) %all-gather.9.cloned.1.call-update) | async-done | bytes 2883600 | tf_op jit(solution)/shard_map/all_gather | solution.py:18
  96.9 48.5 %all-gather.5.cloned.1.call-done = bf16[1024,2048]{1,0:T(8,128)(2,1)} async-done(((bf16[128,2048]{1,0:T(8,128)(2,1)}), bf16[1024,2048]{1,0:T(8,128)(2,1)}) %all-gather.5.cloned.1.call-update) | async-done | bytes 4194320 | tf_op jit(solution)/shard_map/all_gather | solution.py:14
  145.4 11.8 %fusion = f32[1024,1408]{1,0:T(8,128)} fusion(bf16[1024,2048]{1,0:T(8,128)(2,1)} %all-gather.5.cloned.1.call-done, bf16[2048,704]{0,1:T(8,128)(2,1)} %all-gather.9.cloned.1.call-done, bf16[2048,704]{0,1:T(8,128)(2,1)} %all-gather.7.cloned.1.call-done), kind=kOutput, calls=%fused_computation | convolution fusion | flops 5917114368 | bytes 15728640 | tf_op jit(solution)/shard_map/dot_general | solution.py:22
  157.2 30.2 %all-gather.11.cloned.1.call-done = bf16[704,2048]{1,0:T(8,128)(2,1)} async-done(((bf16[704,512]{1,0:T(8,128)(2,1)}), bf16[704,2048]{1,0:T(8,128)(2,1)}) %all-gather.11.cloned.1.call-update) | async-done | bytes 2883600 | tf_op jit(solution)/shard_map/all_gather | solution.py:24
  187.4 10.4 %fusion.5 = f32[1024,2048]{1,0:T(8,128)} fusion(bf16[704,2048]{1,0:T(8,128)(2,1)} %all-gather.11.cloned.1.call-done, f32[1024,1408]{1,0:T(8,128)} %fusion), kind=kOutput, calls=%fused_computation.6 | convolution fusion | flops 2957115392 | bytes 17563648 | tf_op jit(solution)/shard_map/dot_general | solution.py:26
  197.8 0.0 reduce-scatter.2.cloned.1.call-update
  197.8 89.7 %reduce-scatter.2.cloned.1.call-done = f32[128,2048]{1,0:T(8,128)} async-done(((f32[1024,2048]{1,0:T(8,128)}), f32[128,2048]{1,0:T(8,128)}) %reduce-scatter.2.cloned.1.call-update) | async-done | bytes 1048592 | tf_op jit(solution)/shard_map/reduce_scatter | solution.py:25
  287.5 2.1 convert_element_type.15
  (1 shorter events, 0.0 us)
Async XLA Ops:
  6.5 46.9 %all-gather.7.cloned.1.call-start = ((), (), s32[]{:S(2)}) async-start(), calls=%async_computation.2 | async-start | bytes 3604480 | tf_op jit(solution)/shard_map/all_gather | solution.py:17
  7.3 89.6 %all-gather.9.cloned.1.call-start = ((), (), s32[]{:S(2)}) async-start(), calls=%async_computation.3 | async-start | bytes 3604480 | tf_op jit(solution)/shard_map/all_gather | solution.py:18
  8.0 137.3 %all-gather.5.cloned.1.call-start = ((), (), s32[]{:S(2)}) async-start(), calls=%async_computation.1 | async-start | bytes 4718592 | tf_op jit(solution)/shard_map/all_gather | solution.py:14
  11.3 176.1 %all-gather.11.cloned.1.call-start = ((), (), s32[]{:S(2)}) async-start(), calls=%async_computation.4 | async-start | bytes 3604480 | tf_op jit(solution)/shard_map/all_gather | solution.py:24
  11.9 275.6 %reduce-scatter.2.cloned.1.call-start = ((), (), s32[]{:S(2)}) async-start(), calls=%async_computation.5 | async-start | bytes 9437184 | tf_op jit(solution)/shard_map/reduce_scatter | solution.py:25
Sparse Core Ops, SparseCore 0:
  9.2 44.2 all-gather.6
  55.3 41.5 all-gather.8
  98.5 46.8 all-gather.4
  147.0 40.3 all-gather.10
  198.0 89.5 reduce-scatter.1
where the time goes:
time: 296 us
  waiting for transfers between devices  255 us (86%)
  matrix products  22.2 us (8%)
  between operations  13.1 us (4%)
  other arithmetic  5.35 us (2%)
    reduce_scatter x1, waiting for transfers between devices, local(): lax.psum_scatter(jnp.dot(hidden, down_local, preferred_element_type=jnp.f...  89.7 us
    all_gather x1, waiting for transfers between devices, local(): group = lax.all_gather(normed, 'tp', axis=0, tiled=True)  48.5 us
    all_gather x1, waiting for transfers between devices, local(): lax.all_gather(up_weight, 'fs', axis=0, tiled=True)  43.4 us
    all_gather x1, waiting for transfers between devices, local(): lax.all_gather(gate_weight, 'fs', axis=0, tiled=True)  41.5 us
    all_gather x1, waiting for transfers between devices, local(): down_local = lax.all_gather(down_weight, 'fs', axis=1, tiled=True)  30.2 us
    dot_general x1, matrix products, local(): product = jnp.dot(group, joined, preferred_element_type=jnp.float32)  11.8 us
    dot_general x1, matrix products, local(): jnp.dot(hidden, down_local, preferred_element_type=jnp.float32)  10.4 us
  transfers between devices with their start and end apart: 5, of which 5 were waited for; matrix products, arithmetic and copies ran while one was open for 5% of the time, Pallas kernels for 0%

commit v1 on v0

--- a/solution.py
+++ b/solution.py
@@ -11,7 +11,20 @@
     factor = lax.rsqrt(jnp.mean(values * values, axis=-1, keepdims=True) + eps_floor)
     normed = (values * factor * norm_gain).astype(jnp.bfloat16)
     local_ff = gate_weight.shape[1]
-    group = lax.all_gather(normed, "tp", axis=0, tiled=True)
+
+    def take_heads_over_axis(ax_name, x_in):
+        lanes = jax.lax.axis_size(ax_name)
+        part_now = sorted(((q, (q + 1) % lanes) for q in range(lanes)))
+        placed = x_in
+        cards = [placed]
+        for kk in range(1, lanes):
+            placed = jax.lax.ppermute(placed, axis_name=ax_name, perm=part_now)
+            cards.insert(0, placed)
+        aux = jnp.concatenate(cards, axis=0)
+        raw_out = jax.lax.axis_index(ax_name) + 1
+        return jnp.roll(aux, shift=raw_out * x_in.shape[0], axis=0)
+
+    group = take_heads_over_axis("tp", x_in=normed)
     joined = jnp.concatenate(
         (
             lax.all_gather(gate_weight, "fs", axis=0, tiled=True),

time: 296 us -> 249 us (0.84)
  waiting for transfers between devices: 255 us -> 190 us
  local copies, waits for them, and re-layouts: 0 us -> 16 us
    ppermute x0 -> x7, waiting for transfers between devices: none -> 73.6 us  [take_heads_over_axis(): placed = jax.lax.ppermute(placed, axis_name=ax_name, perm=part_now)]
    all_gather x1 -> x0, waiting for transfers between devices: 48.5 us -> none  [local(): group = lax.all_gather(normed, 'tp', axis=0, tiled=True)]
    all_gather x1, waiting for transfers between devices: 43.4 us -> 0.01 us  [local(): lax.all_gather(up_weight, 'fs', axis=0, tiled=True)]
    all_gather x1, waiting for transfers between devices: 41.5 us -> 0.01 us  [local(): lax.all_gather(gate_weight, 'fs', axis=0, tiled=True)]
    unnamed x0 -> x18, local copies, waits for them, and re-layouts: none -> 16 us
    all_gather x1, waiting for transfers between devices: 30.2 us -> 25.2 us  [local(): down_local = lax.all_gather(down_weight, 'fs', axis=1, tiled=True)]
  transfers between devices with their start and end apart: 5 -> 11, of which waited for: 5 -> 9; matrix products, arithmetic and copies ran while one was open for 5% -> 13% of each run, Pallas kernels for 0% -> 0%
where the time goes in v1:
time: 249 us
  waiting for transfers between devices  190 us (76%)
  matrix products  22.6 us (9%)
  local copies, waits for them, and re-layouts  16 us (6%)
  between operations  13.2 us (5%)
  other arithmetic  6.57 us (3%)
    reduce_scatter x1, waiting for transfers between devices, local(): lax.psum_scatter(jnp.dot(hidden, down_local, preferred_element_type=jnp.f...  89.7 us
    ppermute x7, waiting for transfers between devices, take_heads_over_axis(): placed = jax.lax.ppermute(placed, axis_name=ax_name, perm=part_now)  73.6 us
    all_gather x1, waiting for transfers between devices, local(): down_local = lax.all_gather(down_weight, 'fs', axis=1, tiled=True)  25.2 us
    unnamed x18, local copies, waits for them, and re-layouts  16 us
    dot_general x1, matrix products, local(): product = jnp.dot(group, joined, preferred_element_type=jnp.float32)  12.2 us
    dot_general x1, matrix products, local(): jnp.dot(hidden, down_local, preferred_element_type=jnp.float32)  10.4 us
  transfers between devices with their start and end apart: 11, of which 9 were waited for; matrix products, arithmetic and copies ran while one was open for 13% of the time, Pallas kernels for 0%

profile of v1, /device:TPU:0, one launch (start us, length us, event | category | flops | bytes accessed | tf_op | source)
XLA Modules:
  0.0 249.0 jit_solution(5441506715298183775)
XLA Ops:
  6.5 0.0 copy-start
  6.5 0.0 copy-start.1
  6.5 0.0 all-gather.4.cloned.1.call-start
  6.5 0.7 all-gather.4.cloned.1.call-update
  7.3 0.0 all-gather.6.cloned.1.call-start
  7.3 0.7 all-gather.6.cloned.1.call-update
  8.0 0.0 all-gather.8.cloned.1.call-start
  8.1 1.2 fusion.9
  9.3 1.2 fusion.11
  10.5 0.5 collective-permute-start
  11.1 10.9 %collective-permute-done = bf16[128,2048]{1,0:T(8,128)(2,1)S(1)} collective-permute-done((bf16[128,2048]{1,0:T(8,128)(2,1)S(1)}, bf16[128,2048]{1,0:T(8,128)(2,1)S(1)}, u32[]{:S(2)}, u32[]{:S(2)}) %collective-permute-start) | collective-permute-done | bytes 524320 | tf_op jit(solution)/shard_map/ppermute | solution.py:21
  22.0 0.0 collective-permute-start.1
  22.0 10.4 %collective-permute-done.1 = bf16[128,2048]{1,0:T(8,128)(2,1)S(1)} collective-permute-done((bf16[128,2048]{1,0:T(8,128)(2,1)S(1)}, bf16[128,2048]{1,0:T(8,128)(2,1)S(1)}, u32[]{:S(2)}, u32[]{:S(2)}) %collective-permute-start.1) | collective-permute-done | bytes 524320 | tf_op jit(solution)/shard_map/ppermute | solution.py:21
  32.4 0.0 collective-permute-start.2
  32.4 10.4 %collective-permute-done.2 = bf16[128,2048]{1,0:T(8,128)(2,1)S(1)} collective-permute-done((bf16[128,2048]{1,0:T(8,128)(2,1)S(1)}, bf16[128,2048]{1,0:T(8,128)(2,1)S(1)}, u32[]{:S(2)}, u32[]{:S(2)}) %collective-permute-start.2) | collective-permute-done | bytes 524320 | tf_op jit(solution)/shard_map/ppermute | solution.py:21
  42.8 0.0 collective-permute-start.3
  42.8 10.4 %collective-permute-done.3 = bf16[128,2048]{1,0:T(8,128)(2,1)S(1)} collective-permute-done((bf16[128,2048]{1,0:T(8,128)(2,1)S(1)}, bf16[128,2048]{1,0:T(8,128)(2,1)S(1)}, u32[]{:S(2)}, u32[]{:S(2)}) %collective-permute-start.3) | collective-permute-done | bytes 524320 | tf_op jit(solution)/shard_map/ppermute | solution.py:21
  53.2 0.0 collective-permute-start.4
  53.2 10.4 %collective-permute-done.4 = bf16[128,2048]{1,0:T(8,128)(2,1)S(1)} collective-permute-done((bf16[128,2048]{1,0:T(8,128)(2,1)S(1)}, bf16[128,2048]{1,0:T(8,128)(2,1)S(1)}, u32[]{:S(2)}, u32[]{:S(2)}) %collective-permute-start.4) | collective-permute-done | bytes 524320 | tf_op jit(solution)/shard_map/ppermute | solution.py:21
  63.6 0.0 collective-permute-start.5
  63.6 10.5 %collective-permute-done.5 = bf16[128,2048]{1,0:T(8,128)(2,1)} collective-permute-done((bf16[128,2048]{1,0:T(8,128)(2,1)S(1)}, bf16[128,2048]{1,0:T(8,128)(2,1)}, u32[]{:S(2)}, u32[]{:S(2)}) %collective-permute-start.5) | collective-permute-done | bytes 524320 | tf_op jit(solution)/shard_map/ppermute | solution.py:21
  74.1 0.0 collective-permute-start.6
  74.1 0.0 all-gather.8.cloned.1.call-update
  74.1 0.0 reduce-scatter.2.cloned.1.call-start
  74.2 10.6 %collective-permute-done.6 = bf16[128,2048]{1,0:T(8,128)(2,1)} collective-permute-done((bf16[128,2048]{1,0:T(8,128)(2,1)}, bf16[128,2048]{1,0:T(8,128)(2,1)}, u32[]{:S(2)}, u32[]{:S(2)}) %collective-permute-start.6) | collective-permute-done | bytes 524320 | tf_op jit(solution)/shard_map/ppermute | solution.py:21
  84.8 1.9 constant_dynamic-update-slice_fusion.15
  86.7 1.9 constant_dynamic-update-slice_fusion.14
  88.6 0.9 constant_dynamic-update-slice_fusion.13
  89.4 0.8 constant_dynamic-update-slice_fusion.12
  90.3 0.8 constant_dynamic-update-slice_fusion.11
  91.1 0.8 constant_dynamic-update-slice_fusion.10
  92.0 0.8 constant_dynamic-update-slice_fusion.9
  92.8 0.0 copy-done
  92.8 0.0 copy-done.1
  92.8 1.0 constant_dynamic-update-slice_fusion.8
  93.8 1.9 constant_dynamic-update-slice_fusion.7
  95.7 1.9 constant_dynamic-update-slice_fusion.6
  97.6 0.9 constant_dynamic-update-slice_fusion.5
  98.5 0.8 constant_dynamic-update-slice_fusion.4
  99.3 0.8 constant_dynamic-update-slice_fusion.3
  100.1 0.8 constant_dynamic-update-slice_fusion.2
  101.0 0.8 constant_dynamic-update-slice_fusion.1
  101.8 1.0 constant_dynamic-update-slice_fusion
  102.8 0.0 all-gather.4.cloned.1.call-done
  102.8 0.0 all-gather.6.cloned.1.call-done
  102.9 12.2 %fusion = f32[1024,1408]{1,0:T(8,128)} fusion(bf16[2048,704]{0,1:T(8,128)(2,1)} %all-gather.6.cloned.1.call-done, bf16[2048,704]{0,1:T(8,128)(2,1)} %all-gather.4.cloned.1.call-done, bf16[2048,2048]{1,0:T(8,128)(2,1)} %constant_dynamic-update-slice_fusion, s32[]{:T(128)S(6)} %select_n.14), kind=kOutput, calls=%fused_computation | convolution fusion | flops 5917114368 | bytes 15728644 | tf_op jit(solution)/shard_map/dot_general | solution.py:35
  115.0 25.2 %all-gather.8.cloned.1.call-done = bf16[704,2048]{1,0:T(8,128)(2,1)} async-done(((bf16[704,512]{1,0:T(8,128)(2,1)}), bf16[704,2048]{1,0:T(8,128)(2,1)}) %all-gather.8.cloned.1.call-update) | async-done | bytes 2883600 | tf_op jit(solution)/shard_map/all_gather | solution.py:37
  140.3 10.4 %fusion.6 = f32[1024,2048]{1,0:T(8,128)} fusion(bf16[704,2048]{1,0:T(8,128)(2,1)} %all-gather.8.cloned.1.call-done, f32[1024,1408]{1,0:T(8,128)} %fusion), kind=kOutput, calls=%fused_computation.7 | convolution fusion | flops 2957115392 | bytes 17563648 | tf_op jit(solution)/shard_map/dot_general | solution.py:39
  150.7 0.0 reduce-scatter.2.cloned.1.call-update
  150.7 89.7 %reduce-scatter.2.cloned.1.call-done = f32[128,2048]{1,0:T(8,128)} async-done(((f32[1024,2048]{1,0:T(8,128)}), f32[128,2048]{1,0:T(8,128)}) %reduce-scatter.2.cloned.1.call-update) | async-done | bytes 1048592 | tf_op jit(solution)/shard_map/reduce_scatter | solution.py:38
  240.4 2.1 convert_element_type.15
  (1 shorter events, 0.0 us)
Async XLA Ops:
  6.5 86.3 %copy-start = (bf16[128,2048]{1,0:T(8,128)(2,1)S(1)}, bf16[128,2048]{1,0:T(8,128)(2,1)}, u32[]{:S(2)}) copy-start(bf16[128,2048]{1,0:T(8,128)(2,1)} %param.5) | copy-start | bytes 1572868
  6.5 86.3 %copy-start.1 = (f32[2048]{0:T(1024)S(1)}, f32[2048]{0:T(1024)}, u32[]{:S(2)}) copy-start(f32[2048]{0:T(1024)} %param.6) | copy-start | bytes 24580
  6.5 96.3 %all-gather.4.cloned.1.call-start = ((), (), s32[]{:S(2)}) async-start(), calls=%async_computation.1 | async-start | bytes 3604480 | tf_op jit(solution)/shard_map/all_gather | solution.py:30
  7.3 95.6 %all-gather.6.cloned.1.call-start = ((), (), s32[]{:S(2)}) async-start(), calls=%async_computation.2 | async-start | bytes 3604480 | tf_op jit(solution)/shard_map/all_gather | solution.py:31
  8.0 132.2 %all-gather.8.cloned.1.call-start = ((), (), s32[]{:S(2)}) async-start(), calls=%async_computation.3 | async-start | bytes 3604480 | tf_op jit(solution)/shard_map/all_gather | solution.py:37
  10.5 11.4 %collective-permute-start = (bf16[128,2048]{1,0:T(8,128)(2,1)S(1)}, bf16[128,2048]{1,0:T(8,128)(2,1)S(1)}, u32[]{:S(2)}, u32[]{:S(2)}) collective-permute-start(bf16[128,2048]{1,0:T(8,128)(2,1)S(1)} %fusion.11), channel_id=1, source_target_pairs={{0,1},{1,2},{2,3},{3,4},{4,5},{5,6},{6,7},{7,0},{8,9},{9,10},{10,1... | collective-permute-start | bytes 1572872 | tf_op jit(solution)/shard_map/ppermute | solution.py:21
  22.0 10.4 %collective-permute-start.1 = (bf16[128,2048]{1,0:T(8,128)(2,1)S(1)}, bf16[128,2048]{1,0:T(8,128)(2,1)S(1)}, u32[]{:S(2)}, u32[]{:S(2)}) collective-permute-start(bf16[128,2048]{1,0:T(8,128)(2,1)S(1)} %collective-permute-done), channel_id=1, source_target_pairs={{0,1},{1,2},{2,3},{3,4},{4,5},{5,6},{6,7},{7,0},{8,9},{9,10},{10,1... | collective-permute-start | bytes 1572872 | tf_op jit(solution)/shard_map/ppermute | solution.py:21
  32.4 10.4 %collective-permute-start.2 = (bf16[128,2048]{1,0:T(8,128)(2,1)S(1)}, bf16[128,2048]{1,0:T(8,128)(2,1)S(1)}, u32[]{:S(2)}, u32[]{:S(2)}) collective-permute-start(bf16[128,2048]{1,0:T(8,128)(2,1)S(1)} %collective-permute-done.1), channel_id=1, source_target_pairs={{0,1},{1,2},{2,3},{3,4},{4,5},{5,6},{6,7},{7,0},{8,9},{9,10},{10,1... | collective-permute-start | bytes 1572872 | tf_op jit(solution)/shard_map/ppermute | solution.py:21
  42.8 10.4 %collective-permute-start.3 = (bf16[128,2048]{1,0:T(8,128)(2,1)S(1)}, bf16[128,2048]{1,0:T(8,128)(2,1)S(1)}, u32[]{:S(2)}, u32[]{:S(2)}) collective-permute-start(bf16[128,2048]{1,0:T(8,128)(2,1)S(1)} %collective-permute-done.2), channel_id=1, source_target_pairs={{0,1},{1,2},{2,3},{3,4},{4,5},{5,6},{6,7},{7,0},{8,9},{9,10},{10,1... | collective-permute-start | bytes 1572872 | tf_op jit(solution)/shard_map/ppermute | solution.py:21
  53.2 10.4 %collective-permute-start.4 = (bf16[128,2048]{1,0:T(8,128)(2,1)S(1)}, bf16[128,2048]{1,0:T(8,128)(2,1)S(1)}, u32[]{:S(2)}, u32[]{:S(2)}) collective-permute-start(bf16[128,2048]{1,0:T(8,128)(2,1)S(1)} %collective-permute-done.3), channel_id=1, source_target_pairs={{0,1},{1,2},{2,3},{3,4},{4,5},{5,6},{6,7},{7,0},{8,9},{9,10},{10,1... | collective-permute-start | bytes 1572872 | tf_op jit(solution)/shard_map/ppermute | solution.py:21
  63.6 10.5 %collective-permute-start.5 = (bf16[128,2048]{1,0:T(8,128)(2,1)S(1)}, bf16[128,2048]{1,0:T(8,128)(2,1)}, u32[]{:S(2)}, u32[]{:S(2)}) collective-permute-start(bf16[128,2048]{1,0:T(8,128)(2,1)S(1)} %collective-permute-done.4), channel_id=1, source_target_pairs={{0,1},{1,2},{2,3},{3,4},{4,5},{5,6},{6,7},{7,0},{8,9},{9,10},{10,1... | collective-permute-start | bytes 1572872 | tf_op jit(solution)/shard_map/ppermute | solution.py:21
  74.1 10.7 %collective-permute-start.6 = (bf16[128,2048]{1,0:T(8,128)(2,1)}, bf16[128,2048]{1,0:T(8,128)(2,1)}, u32[]{:S(2)}, u32[]{:S(2)}) collective-permute-start(bf16[128,2048]{1,0:T(8,128)(2,1)} %collective-permute-done.5), channel_id=1, source_target_pairs={{0,1},{1,2},{2,3},{3,4},{4,5},{5,6},{6,7},{7,0},{8,9},{9,10},{10,1... | collective-permute-start | bytes 1572872 | tf_op jit(solution)/shard_map/ppermute | solution.py:21
  74.1 166.2 %reduce-scatter.2.cloned.1.call-start = ((), (), s32[]{:S(2)}) async-start(), calls=%async_computation.4 | async-start | bytes 9437184 | tf_op jit(solution)/shard_map/reduce_scatter | solution.py:38
Sparse Core Ops, SparseCore 0:
  9.2 44.2 all-gather.3
  55.3 41.5 all-gather.5
  98.7 41.5 all-gather.7
  150.8 89.5 reduce-scatter.1
